TPU v7x, 32 devices: a whole 2x2x4 slice. The times are simulated.
32 devices in a mesh: kv: 16 (over z, y, x), tp: 2 (over core).
Axes of the slice: x: 2, y: 2, z: 4, core: 2. Of those that a mesh axis runs over, the one named last changes fastest.
Arguments:
- tokens: bfloat16 [24, 4096], P(None, 'kv'), may hold values from -60 to 60
- gain_first: bfloat16 [4096], P('kv'), may hold values from 0.099609375 to 1.8984375
- gate_first: bfloat16 [4096, 11264], P('kv', 'tp'), may hold values from -0.09375 to 0.09375
- up_first: bfloat16 [4096, 11264], P('kv', 'tp'), may hold values from -0.09375 to 0.09375
- down_first: bfloat16 [11264, 4096], P('tp', 'kv'), may hold values from -0.0546875 to 0.0546875
- gain_mixer: bfloat16 [4096], P('kv'), may hold values from 0.099609375 to 1.8984375
- query_weight: bfloat16 [4096, 2048], P('kv', 'tp'), may hold values from -0.09375 to 0.09375
- key_weight: bfloat16 [4096, 2048], P('kv', 'tp'), may hold values from -0.25 to 0.25
- value_weight: bfloat16 [4096, 2048], P('kv', 'tp'), may hold values from -0.09375 to 0.09375
- forget_weight: bfloat16 [4096, 16], replicated, may hold values from -0.09375 to 0.09375
- forget_bias: float32 [16], replicated, may hold values from -1 to 2
- key_cache: bfloat16 [24, 8192, 16, 128], P(None, 'kv', 'tp'), may hold values from -2000 to 2000
- value_cache: bfloat16 [24, 8192, 16, 128], P(None, 'kv', 'tp'), may hold values from -6 to 6
- forget_sum: float32 [24, 16, 8192], P(None, 'tp', 'kv'), may hold values from -1024 to 0, as said below
- out_weight: bfloat16 [2048, 4096], P('tp', 'kv'), may hold values from -0.5 to 0.5
- gain_second: bfloat16 [4096], P('kv'), may hold values from 0.099609375 to 1.8984375
- gate_second: bfloat16 [4096, 11264], P('kv', 'tp'), may hold values from -0.09375 to 0.09375
- up_second: bfloat16 [4096, 11264], P('kv', 'tp'), may hold values from -0.09375 to 0.09375
- down_second: bfloat16 [11264, 4096], P('tp', 'kv'), may hold values from -0.0546875 to 0.0546875
Outputs:
- updated: bfloat16 [24, 4096], P(None, 'kv')
Inputs may be any that keep to these rules, and one draw needn't show every extreme that they name: forget_sum[b, h, s] is the sum of the log forget gates of the cached positions after s, up to the last cached one, for sequence b and head h; it never falls with s, is at most 0, and rises to 0 at the last cached position.
All inputs are finite; a program needn't handle non-finite values.
Results may differ from a plain program's by a relative error of at most 0.02.
Values may be sent and summed in bfloat16 or wider, within the bound.
A program may use at most 128 MiB of HBM per device.

v0:
```python
import jax
import jax.numpy as jnp
from jax import lax
from jax.sharding import PartitionSpec as P

D = 4096
BLOCK = 128


EPSILON = 1e-06


def combined_all(value, axis, combine):
    everything = jax.tree.map(lambda part: lax.all_gather(part, axis), value)
    initial = jax.tree.map(lambda part: part[0], everything)

    def turn(k, so_far):
        return combine(so_far, jax.tree.map(lambda part: part[k], everything))

    return lax.fori_loop(1, lax.axis_size(axis), turn, initial)


def merge_parts(former, latter):
    highest = jnp.maximum(former[0], latter[0])
    left_scale = jnp.exp(former[0] - highest)
    right_scale = jnp.exp(latter[0] - highest)
    return (
        highest,
        former[1] * left_scale + latter[1] * right_scale,
        former[2] * left_scale[..., None] + latter[2] * right_scale[..., None],
    )


def row_factor(squares):
    return lax.rsqrt(squares / D + EPSILON)[:, None]


def feed_forward(tokens, norm_gain, gate_matrix, up_matrix, down_matrix):
    widened = tokens.astype(jnp.float32)
    squares = jnp.sum(widened * widened, axis=1)
    scaled = (widened * norm_gain.astype(jnp.float32)).astype(jnp.bfloat16)
    products = jnp.stack(
        [
            jnp.dot(scaled, gate_matrix, preferred_element_type=jnp.float32),
            jnp.dot(scaled, up_matrix, preferred_element_type=jnp.float32),
        ]
    )
    products, squares = lax.psum((products, squares), "kv")
    factor = row_factor(squares)
    hidden = (jax.nn.silu(factor * products[0]) * (factor * products[1])).astype(jnp.bfloat16)
    partial_value = jnp.dot(hidden, down_matrix, preferred_element_type=jnp.float32)
    summed = lax.psum(partial_value.astype(jnp.bfloat16), "tp").astype(jnp.float32)
    return (widened + 0.5 * summed).astype(jnp.bfloat16)


def mix_tokens(
    tokens,
    norm_gain,
    query_weight,
    key_weight,
    value_weight,
    forget_weight,
    forget_bias,
    key_cache,
    value_cache,
    forget_sum,
    out_weight,
):
    widened = tokens.astype(jnp.float32)
    squares = jnp.sum(widened * widened, axis=1)
    scaled = (widened * norm_gain.astype(jnp.float32)).astype(jnp.bfloat16)
    columns = scaled.shape[1]
    forget_rows = lax.dynamic_slice_in_dim(
        forget_weight, lax.axis_index("kv") * columns, columns, 0
    )
    triple = jnp.stack(
        [
            jnp.dot(scaled, query_weight, preferred_element_type=jnp.float32),
            jnp.dot(scaled, key_weight, preferred_element_type=jnp.float32),
            jnp.dot(scaled, value_weight, preferred_element_type=jnp.float32),
        ]
    )
    gate_terms = jnp.dot(scaled, forget_rows, preferred_element_type=jnp.float32)
    triple, gate_terms, squares = lax.psum((triple, gate_terms, squares), "kv")
    factor = row_factor(squares)
    seq_count = tokens.shape[0]
    local_heads = key_cache.shape[2]
    head_size = key_cache.shape[3]
    shaped = (
        (factor[None] * triple).astype(jnp.bfloat16).reshape(3, seq_count, local_heads, head_size)
    )
    query_rows, new_key, new_value = (shaped[0], shaped[1], shaped[2])
    all_gates = jax.nn.log_sigmoid(factor * gate_terms + forget_bias)
    log_gate = lax.dynamic_slice_in_dim(
        all_gates, lax.axis_index("tp") * local_heads, local_heads, 1
    )
    inverse = head_size ** (-0.5)
    scores = (
        jnp.einsum("bhd,bshd->bhs", query_rows, key_cache, preferred_element_type=jnp.float32)
        * inverse
    )
    scores = scores + forget_sum + log_gate[:, :, None]
    blocks = key_cache.shape[1] // BLOCK
    scores = scores.reshape(seq_count, local_heads, blocks, BLOCK)
    highest = jnp.max(scores, axis=3)
    weights = jnp.exp(scores - highest[..., None]).astype(jnp.bfloat16)
    block_sum = jnp.sum(weights.astype(jnp.float32), axis=3)
    block_value = jnp.einsum(
        "bhcs,bcshd->bhcd",
        weights,
        value_cache.reshape(seq_count, blocks, BLOCK, local_heads, head_size),
        preferred_element_type=jnp.float32,
    )
    local_top = jnp.max(highest, axis=2)
    rescale = jnp.exp(highest - local_top[..., None])
    denominator = jnp.sum(rescale * block_sum, axis=2)
    numerator = jnp.sum(rescale[..., None] * block_value, axis=2)
    local_top, denominator, numerator = combined_all(
        (local_top, denominator, numerator), "kv", merge_parts
    )
    own_score = (
        jnp.sum(query_rows.astype(jnp.float32) * new_key.astype(jnp.float32), axis=2) * inverse
    )
    ceiling = jnp.maximum(local_top, own_score)
    cache_scale = jnp.exp(local_top - ceiling)
    own_scale = jnp.exp(own_score - ceiling)
    attended = (
        (numerator * cache_scale[..., None] + own_scale[..., None] * new_value.astype(jnp.float32))
        / (denominator * cache_scale + own_scale)[..., None]
    ).astype(jnp.bfloat16)
    partial_value = jnp.dot(
        attended.reshape(seq_count, local_heads * head_size),
        out_weight,
        preferred_element_type=jnp.float32,
    )
    summed = lax.psum(partial_value.astype(jnp.bfloat16), "tp").astype(jnp.float32)
    return (widened + summed).astype(jnp.bfloat16)


def on_device(
    tokens,
    gain_first,
    gate_first,
    up_first,
    down_first,
    gain_mixer,
    query_weight,
    key_weight,
    value_weight,
    forget_weight,
    forget_bias,
    key_cache,
    value_cache,
    forget_sum,
    out_weight,
    gain_second,
    gate_second,
    up_second,
    down_second,
):
    first_out = feed_forward(tokens, gain_first, gate_first, up_first, down_first)
    mixed = mix_tokens(
        first_out,
        gain_mixer,
        query_weight,
        key_weight,
        value_weight,
        forget_weight,
        forget_bias,
        key_cache,
        value_cache,
        forget_sum,
        out_weight,
    )
    return feed_forward(mixed, gain_second, gate_second, up_second, down_second)


def solution(mesh):
    in_specs = (
        P(None, "kv"),
        P("kv"),
        P("kv", "tp"),
        P("kv", "tp"),
        P("tp", "kv"),
        P("kv"),
        P("kv", "tp"),
        P("kv", "tp"),
        P("kv", "tp"),
        P(),
        P(),
        P(None, "kv", "tp", None),
        P(None, "kv", "tp", None),
        P(None, "tp", "kv"),
        P("tp", "kv"),
        P("kv"),
        P("kv", "tp"),
        P("kv", "tp"),
        P("tp", "kv"),
    )
    out_specs = P(None, "kv")
    return jax.shard_map(
        on_device, mesh=mesh, in_specs=in_specs, out_specs=out_specs, check_vma=False
    )
```

profile of v0, /device:TPU:0, one launch (start us, length us, event | category | flops | bytes accessed | tf_op | source)
XLA Modules:
  0.0 537.3 jit_solution(9144958577285761206)
XLA Ops:
  8.4 1.2 convolution_bitcast_fusion.2
  10.1 1.1 pad_maximum_fusion
  11.4 43.9 %psum.70 = f32[24]{0:T(128)S(1)} all-reduce(f32[24]{0:T(128)S(1)} %fusion.32), channel_id=1, replica_groups=mesh['kv'=16,'tp'=2] {'kv'}, use_global_device_ids=true, to_apply=%region_1.0 | all-reduce | flops 24 | bytes 192 | tf_op jit(solution)/shard_map/psum | solution.py:48
  55.3 73.5 %all-reduce.5.cloned.1.call-done = f32[2,24,5632]{2,1,0:T(8,128)} async-done(((f32[2,24,5632]{2,1,0:T(8,128)}), f32[2,24,5632]{2,1,0:T(8,128)}) %all-reduce.5.cloned.1.call-update) | async-done | bytes 1081360 | tf_op jit(solution)/shard_map/psum | solution.py:48
  128.8 2.7 convolution_convert_fusion.1
  131.5 3.3 psum.72
  135.7 41.1 %all-reduce = (f32[24]{0:T(128)S(1)}, f32[24,16]{0,1:T(8,128)S(1)}) all-reduce(f32[24]{0:T(128)S(1)} %get-tuple-element.217, f32[24,16]{0,1:T(8,128)S(1)} %fusion.45), channel_id=1, replica_groups=mesh['kv'=16,'tp'=2] {'kv'}, use_global_device_ids=true, to_apply=%region_5.6 | all-reduce | flops 408 | bytes 3264 | tf_op jit(solution)/shard_map/psum | solution.py:84
  178.4 104.0 %all-reduce.7.cloned.1.call-done = f32[3,24,1024]{2,1,0:T(8,128)} async-done(((f32[3,24,1024]{2,1,0:T(8,128)}), f32[3,24,1024]{2,1,0:T(8,128)}) %all-reduce.7.cloned.1.call-update) | async-done | bytes 294928 | tf_op jit(solution)/shard_map/psum | solution.py:84
  282.4 1.0 multiply_convert_fusion
  283.5 11.6 %fusion.5 = f32[24,8,1,512]{3,2,1,0:T(1,128)S(1)} fusion(bf16[24,8,128,1]{2,3,1,0:T(2,128)(2,1)S(1)} %reshape.67, bf16[24,512,8,128]{3,2,1,0:T(8,128)(2,1)} %param.32), kind=kOutput, calls=%fused_computation.10 | convolution fusion | flops 25165824 | bytes 25608192 | tf_op jit(solution)/shard_map/bhd,bshd->bhs/dot_general | solution.py:99
  296.0 11.4 %fusion.3 = f32[24,8,4,1,128]{4,3,2,1,0:T(1,128)S(1)} fusion(bf16[24,4,128,8,128]{4,3,2,1,0:T(8,128)(2,1)} %bitcast.137, bf16[24,8,4,128,1]{3,1,2,0,4:T(8,128)(2,1)S(1)} %get-tuple-element.219), kind=kOutput, calls=%fused_computation.8 | convolution fusion | flops 25165824 | bytes 25755648 | tf_op jit(solution)/shard_map/bhcs,bcshd->bhcd/dot_general | solution.py:108
  308.7 39.2 %all-gather.4 = f32[16,24,8]{1,2,0:T(8,128)S(1)} all-gather(f32[1,24,8]{1,2,0:T(8,128)S(1)} %copy.49), channel_id=3, replica_groups=mesh['kv'=16,'tp'=2] {'kv'}, dimensions={0}, use_global_device_ids=true | all-gather | bytes 13056 | tf_op jit(solution)/shard_map/all_gather | solution.py:14
  347.9 35.9 %all-gather.3 = f32[16,24,8]{1,2,0:T(8,128)S(1)} all-gather(f32[1,24,8]{1,2,0:T(8,128)S(1)} %copy.48), channel_id=2, replica_groups=mesh['kv'=16,'tp'=2] {'kv'}, dimensions={0}, use_global_device_ids=true | all-gather | bytes 13056 | tf_op jit(solution)/shard_map/all_gather | solution.py:14
  384.8 18.4 %while.19 = (s32[]{:T(128)}, f32[24,8]{0,1:T(8,128)S(1)}, f32[24,8]{0,1:T(8,128)S(1)}, f32[24,8,128]{2,1,0:T(8,128)S(1)}, f32[16,24,8]{1,2,0:T(8,128)S(1)}, /*in...) while((s32[]{:T(128)}, f32[24,8]{0,1:T(8,128)S(1)}, ...), condition=%wide.region_14.15_spmd, body=%wide.region_13.14_spmd.sunk | while | flops 74885 | bytes 305807 | solution.py:20
  385.0 1.0 fusion.82
  387.4 1.0 fusion.82
  388.6 1.0 fusion.82
  389.9 1.0 fusion.82
  391.1 1.0 fusion.82
  394.8 1.0 fusion.82
  396.0 1.0 fusion.82
  397.2 1.0 fusion.82
  398.4 1.0 fusion.82
  399.7 1.0 fusion.82
  403.7 3.3 psum.76
  407.1 2.3 convolution_bitcast_fusion.1
  409.4 2.3 convolution_bitcast_fusion
  411.7 1.1 pad_maximum_fusion.1
  412.9 39.2 %psum.77 = f32[24]{0:T(128)S(1)} all-reduce(f32[24]{0:T(128)S(1)} %get-tuple-element.206), channel_id=1, replica_groups=mesh['kv'=16,'tp'=2] {'kv'}, use_global_device_ids=true, to_apply=%region_18.19 | all-reduce | flops 24 | bytes 192 | tf_op jit(solution)/shard_map/psum | solution.py:48
  452.1 72.0 %all-reduce.9.cloned.1.call-done = f32[2,24,5632]{2,1,0:T(8,128)} async-done(((f32[2,24,5632]{2,1,0:T(8,128)}), f32[2,24,5632]{2,1,0:T(8,128)}) %all-reduce.9.cloned.1.call-update) | async-done | bytes 1081360 | tf_op jit(solution)/shard_map/psum | solution.py:48
  524.1 2.7 convolution_convert_fusion
  526.8 3.3 psum.79
  (125 shorter events, 17.0 us)
Async XLA Ops:
  6.5 1.8 copy-start
  6.5 3.0 copy-start.8
  6.5 122.2 %all-reduce.5.cloned.1.call-start = ((), (), s32[]{:S(2)}) async-start(), calls=%async_computation | async-start | bytes 2162688 | tf_op jit(solution)/shard_map/psum | solution.py:48
  6.5 3.0 copy-start.2
  9.6 1.7 copy-start.10
  11.2 165.6 %copy-start.3 = (bf16[256,1024]{1,0:T(8,128)(2,1)S(1)}, bf16[256,1024]{1,0:T(8,128)(2,1)}, u32[]{:S(2)}) copy-start(bf16[256,1024]{1,0:T(8,128)(2,1)} %param.29) | copy-start | bytes 1572868
  11.2 165.8 %copy-start.4 = (bf16[256,1024]{1,0:T(8,128)(2,1)S(1)}, bf16[256,1024]{1,0:T(8,128)(2,1)}, u32[]{:S(2)}) copy-start(bf16[256,1024]{1,0:T(8,128)(2,1)} %param.27) | copy-start | bytes 1572868
  11.2 271.2 %all-reduce.7.cloned.1.call-start = ((), (), s32[]{:S(2)}) async-start(), calls=%async_computation.1 | async-start | bytes 589824 | tf_op jit(solution)/shard_map/psum | solution.py:84
  55.3 121.9 %copy-start.5 = (bf16[256,1024]{1,0:T(8,128)(2,1)S(1)}, bf16[256,1024]{1,0:T(8,128)(2,1)}, u32[]{:S(2)}) copy-start(bf16[256,1024]{1,0:T(8,128)(2,1)} %param.28) | copy-start | bytes 1572868
  55.3 122.9 %copy-start.9 = (f32[16]{0:T(128)S(1)}, f32[16]{0:T(128)}, u32[]{:S(2)}) copy-start(f32[16]{0:T(128)} %param.31) | copy-start | bytes 196
  178.2 205.7 %all-gather.7.cloned.1.call-start = ((), (), s32[]{:S(2)}) async-start(), calls=%async_computation.3 | async-start | bytes 1671168 | tf_op jit(solution)/shard_map/all_gather | solution.py:14
  283.5 11.6 %copy-start.7 = (f32[24,8,512]{2,1,0:T(8,128)S(1)}, f32[24,8,512]{2,1,0:T(8,128)}, u32[]{:S(2)}) copy-start(f32[24,8,512]{2,1,0:T(8,128)} %param.34) | copy-start | bytes 1179652
  296.0 12.3 %copy-start.11 = (bf16[256]{0:T(256)(128)(2,1)S(1)}, bf16[256]{0:T(256)(128)(2,1)}, u32[]{:S(2)}) copy-start(bf16[256]{0:T(256)(128)(2,1)} %param.36) | copy-start | bytes 1540
  307.4 96.1 %copy-start.6 = (bf16[1024,256]{1,0:T(8,128)(2,1)S(1)}, bf16[1024,256]{1,0:T(8,128)(2,1)}, u32[]{:S(2)}) copy-start(bf16[1024,256]{1,0:T(8,128)(2,1)} %param.35) | copy-start | bytes 1572868
  308.3 215.9 %all-reduce.9.cloned.1.call-start = ((), (), s32[]{:S(2)}) async-start(), calls=%async_computation.2 | async-start | bytes 2162688 | tf_op jit(solution)/shard_map/psum | solution.py:48
  412.9 117.9 %copy-start.1 = (bf16[256,5632]{1,0:T(8,128)(2,1)S(1)}, bf16[256,5632]{1,0:T(8,128)(2,1)}, u32[]{:S(2)}) copy-start(bf16[256,5632]{1,0:T(8,128)(2,1)} %param.24) | copy-start | bytes 8650756
Sparse Core Ops, SparseCore 0:
  12.9 115.8 all-reduce.4
  178.3 104.0 all-reduce.6
  308.4 57.5 all-gather.6
  413.0 111.0 all-reduce.8
where the time goes:
time: 538 us; the launch traced here: 537 us
  waiting for transfers between devices  250 us (46%)
  blocking collectives  209 us (39%)
  matrix products  36.3 us (7%)
  other arithmetic  23.5 us (4%)
  between operations  13.4 us (2%)
    psum x2, waiting for transfers between devices, feed_forward(): products, squares = lax.psum((products, squares), 'kv')  146 us
    psum x1, waiting for transfers between devices, mix_tokens(): triple, gate_terms, squares = lax.psum((triple, gate_terms, squares), 'kv')  104 us
    psum x2, blocking collectives, feed_forward(): products, squares = lax.psum((products, squares), 'kv')  83.1 us
    all_gather x2, blocking collectives, combined_all(): everything = jax.tree.map(lambda part: lax.all_gather(part, axis), value)  75.2 us
    psum x1, blocking collectives, mix_tokens(): triple, gate_terms, squares = lax.psum((triple, gate_terms, squares), 'kv')  41.1 us
    add x15, other arithmetic, merge_parts(): former[2] * left_scale[..., None] + latter[2] * right_scale[..., None]  15.4 us
    dot_general x1, matrix products, mix_tokens(): jnp.einsum('bhd,bshd->bhs', query_rows, key_cache, preferred_element_type...  11.6 us
    dot_general x1, matrix products, mix_tokens(): jnp.einsum('bhcs,bcshd->bhcd', weights, value_cache.reshape(seq_count, bl...  11.4 us
  transfers between devices with their start and end apart: 4, of which 3 were waited for; matrix products, arithmetic and copies ran while one was open for 0% of the time, Pallas kernels for 0%

commit v1 on v0

v1 whole, which is shorter than its diff:
```python
import functools

import jax
import jax.numpy as jnp
from jax import lax
from jax.experimental import pallas as pl
from jax.experimental.pallas import tpu as pltpu
from jax.sharding import PartitionSpec as P

EPSILON = 1e-06
LANES = 128
F32 = jnp.float32
BF16 = jnp.bfloat16


def chunk_width(columns, devices):
    tiles = -(-columns // LANES)
    return LANES * (-(-tiles // devices))


def greet(n_kv, n_tp):
    me, core = lax.axis_index("kv"), lax.axis_index("tp")
    barrier = pltpu.get_barrier_semaphore()

    def along_kv(k, carry):
        pl.semaphore_signal(
            barrier, inc=1, device_id={"kv": lax.rem(me + k, n_kv)},
            device_id_type=pl.DeviceIdType.MESH,
        )
        return carry

    lax.fori_loop(1, n_kv, along_kv, 0)
    for k in range(1, n_tp):
        pl.semaphore_signal(
            barrier, inc=1, device_id={"tp": lax.rem(core + k, n_tp)},
            device_id_type=pl.DeviceIdType.MESH,
        )
    pl.semaphore_wait(barrier, n_kv - 1 + n_tp - 1)


def remote(source, target, send_sem, recv_sem, axis, peer):
    return pltpu.make_async_remote_copy(
        src_ref=source, dst_ref=target, send_sem=send_sem, recv_sem=recv_sem,
        device_id={axis: peer}, device_id_type=pl.DeviceIdType.MESH,
    )


def share(buffer, send_sems, recv_sems, axis, count):
    me = lax.axis_index(axis)

    def send(k, carry):
        peer = lax.rem(me + k, count)
        remote(buffer.at[me], buffer.at[me], send_sems.at[peer], recv_sems.at[me], axis, peer).start()
        return carry

    lax.fori_loop(1, count, send, 0)


def shared_from(buffer, send_sems, recv_sems, axis, peer):
    me = lax.axis_index(axis)
    remote(buffer.at[me], buffer.at[peer], send_sems.at[peer], recv_sems.at[peer], axis, peer).wait_recv()


def drain(buffer, send_sems, recv_sems, axis, count):
    me = lax.axis_index(axis)

    def done(k, carry):
        peer = lax.rem(me + k, count)
        remote(buffer.at[me], buffer.at[me], send_sems.at[peer], recv_sems.at[me], axis, peer).wait_send()
        return carry

    lax.fori_loop(1, count, done, 0)


def collect(buffer, send_sems, recv_sems, axis, count):
    me = lax.axis_index(axis)

    def arrived(k, carry):
        shared_from(buffer, send_sems, recv_sems, axis, lax.rem(me + k, count))
        return carry

    lax.fori_loop(1, count, arrived, 0)


def total_over(buffer, count):
    def add(j, so_far):
        return so_far + buffer[j].astype(F32)

    return lax.fori_loop(1, count, add, buffer[0].astype(F32))


def across_tp(part, tp_buf, send_sems, recv_sems, n_tp):
    tp_buf[lax.axis_index("tp")] = part.astype(BF16)
    share(tp_buf, send_sems, recv_sems, "tp", n_tp)
    collect(tp_buf, send_sems, recv_sems, "tp", n_tp)
    return total_over(tp_buf, n_tp)


def feed_kernel(
    n_kv, n_tp, width, d_total,
    tokens_ref, gain_ref, gate_hbm, up_hbm, down_hbm, out_ref,
    gate_v, up_v, down_v, stat, send, recv, hid, tp_buf,
    w_sems, stat_s, stat_r, rs_s, rs_r, ag_s, ag_r, tp_s, tp_r,
):
    me = lax.axis_index("kv")
    hidden_units = gate_hbm.shape[1]
    loads = [
        pltpu.make_async_copy(gate_hbm, gate_v.at[:, pl.ds(0, hidden_units)], w_sems.at[0]),
        pltpu.make_async_copy(up_hbm, up_v.at[:, pl.ds(0, hidden_units)], w_sems.at[1]),
        pltpu.make_async_copy(down_hbm, down_v.at[pl.ds(0, hidden_units)], w_sems.at[2]),
    ]
    for load in loads:
        load.start()
    padded = gate_v.shape[1]
    if padded > hidden_units:
        gate_v[:, hidden_units:] = jnp.zeros((gate_v.shape[0], padded - hidden_units), BF16)
        up_v[:, hidden_units:] = jnp.zeros((gate_v.shape[0], padded - hidden_units), BF16)
        down_v[hidden_units:, :] = jnp.zeros((padded - hidden_units, down_v.shape[1]), BF16)
    widened = tokens_ref[...].astype(F32)
    scaled = (widened * gain_ref[...].astype(F32)).astype(BF16)
    rows = widened.shape[0]
    stat[me] = jnp.broadcast_to(jnp.sum(widened * widened, axis=1, keepdims=True), (rows, LANES))
    greet(n_kv, n_tp)
    share(stat, stat_s, stat_r, "kv", n_kv)
    loads[0].wait()
    loads[1].wait()

    def partial(j):
        columns = pl.ds(pl.multiple_of(j * width, LANES), width)
        return (
            jnp.dot(scaled, gate_v[:, columns], preferred_element_type=F32),
            jnp.dot(scaled, up_v[:, columns], preferred_element_type=F32),
        )

    def spread(k, carry):
        peer = lax.rem(me + k, n_kv)
        gate_part, up_part = partial(peer)
        send[peer, :, :width] = gate_part.astype(BF16)
        send[peer, :, width:] = up_part.astype(BF16)
        remote(send.at[peer], recv.at[me], rs_s.at[peer], rs_r.at[me], "kv", peer).start()
        return carry

    lax.fori_loop(1, n_kv, spread, 0)
    own = jnp.concatenate(partial(me), axis=1)
    collect(stat, stat_s, stat_r, "kv", n_kv)
    factor = lax.rsqrt(total_over(stat, n_kv)[:, :1] / d_total + EPSILON)

    def gather(k, so_far):
        peer = lax.rem(me + k, n_kv)
        remote(send.at[peer], recv.at[peer], rs_s.at[peer], rs_r.at[peer], "kv", peer).wait_recv()
        return so_far + recv[peer].astype(F32)

    both = lax.fori_loop(1, n_kv, gather, own)
    gate_value = factor * both[:, :width]
    up_value = factor * both[:, width:]
    hid[me] = (gate_value / (1.0 + jnp.exp(-gate_value)) * up_value).astype(BF16)
    share(hid, ag_s, ag_r, "kv", n_kv)
    loads[2].wait()

    def down(j):
        return jnp.dot(
            hid[j], down_v[pl.ds(pl.multiple_of(j * width, LANES), width), :],
            preferred_element_type=F32,
        )

    def further(k, so_far):
        peer = lax.rem(me + k, n_kv)
        shared_from(hid, ag_s, ag_r, "kv", peer)
        return so_far + down(peer)

    part = lax.fori_loop(1, n_kv, further, down(me))
    summed = across_tp(part, tp_buf, tp_s, tp_r, n_tp)
    out_ref[...] = (widened + 0.5 * summed).astype(BF16)

    def sent(k, carry):
        peer = lax.rem(me + k, n_kv)
        remote(send.at[peer], recv.at[me], rs_s.at[peer], rs_r.at[me], "kv", peer).wait_send()
        return carry

    lax.fori_loop(1, n_kv, sent, 0)
    drain(stat, stat_s, stat_r, "kv", n_kv)
    drain(hid, ag_s, ag_r, "kv", n_kv)
    drain(tp_buf, tp_s, tp_r, "tp", n_tp)


VM = pl.BlockSpec(memory_space=pltpu.VMEM)
ANY = pl.BlockSpec(memory_space=pl.ANY)
DMA = pltpu.SemaphoreType.DMA


def feed_forward(tokens, gain, gate, up, down, identity):
    n_kv, n_tp = lax.axis_size("kv"), lax.axis_size("tp")
    rows, features = tokens.shape
    hidden_units = gate.shape[1]
    width = chunk_width(hidden_units, n_kv)
    padded = width * n_kv
    return pl.pallas_call(
        functools.partial(feed_kernel, n_kv, n_tp, width, float(features * n_kv)),
        out_shape=jax.ShapeDtypeStruct((rows, features), BF16),
        in_specs=[VM, VM, ANY, ANY, ANY],
        out_specs=VM,
        scratch_shapes=[
            pltpu.VMEM((features, padded), BF16),
            pltpu.VMEM((features, padded), BF16),
            pltpu.VMEM((padded, features), BF16),
            pltpu.VMEM((n_kv, rows, LANES), F32),
            pltpu.VMEM((n_kv, rows, 2 * width), BF16),
            pltpu.VMEM((n_kv, rows, 2 * width), BF16),
            pltpu.VMEM((n_kv, rows, width), BF16),
            pltpu.VMEM((n_tp, rows, features), BF16),
            DMA((3,)),
            DMA((n_kv,)), DMA((n_kv,)),
            DMA((n_kv,)), DMA((n_kv,)),
            DMA((n_kv,)), DMA((n_kv,)),
            DMA((n_tp,)), DMA((n_tp,)),
        ],
        compiler_params=pltpu.CompilerParams(
            collective_id=identity, has_side_effects=True, vmem_limit_bytes=32 << 20
        ),
        name=f"feed_{identity}",
    )(tokens, gain.reshape(1, features), gate, up, down)


def project_kernel(
    n_kv, n_tp, width, d_total,
    tokens_ref, gain_ref, query_hbm, key_hbm, value_hbm, forget_ref, bias_ref, out_ref, gates_ref,
    w_v, stat, send, recv, mine,
    w_sems, stat_s, stat_r, rs_s, rs_r, ag_s, ag_r,
):
    me = lax.axis_index("kv")
    each = query_hbm.shape[1]
    loads = [
        pltpu.make_async_copy(part, w_v.at[:, pl.ds(i * each, each)], w_sems.at[i])
        for i, part in enumerate((query_hbm, key_hbm, value_hbm))
    ]
    for load in loads:
        load.start()
    padded = w_v.shape[1]
    if padded > 3 * each:
        w_v[:, 3 * each :] = jnp.zeros((w_v.shape[0], padded - 3 * each), BF16)
    widened = tokens_ref[...].astype(F32)
    scaled = (widened * gain_ref[...].astype(F32)).astype(BF16)
    rows, features = widened.shape
    heads = forget_ref.shape[1]
    forget_rows = forget_ref[pl.ds(pl.multiple_of(me * features, features), features), :]
    stat[me, 0] = jnp.broadcast_to(jnp.sum(widened * widened, axis=1, keepdims=True), (rows, LANES))
    stat[me, 1] = jnp.zeros((rows, LANES), F32)
    stat[me, 1, :, :heads] = jnp.dot(scaled, forget_rows, preferred_element_type=F32)
    greet(n_kv, 1)
    share(stat, stat_s, stat_r, "kv", n_kv)
    for load in loads:
        load.wait()

    def partial(j):
        columns = pl.ds(pl.multiple_of(j * width, LANES), width)
        return jnp.dot(scaled, w_v[:, columns], preferred_element_type=F32)

    def spread(k, carry):
        peer = lax.rem(me + k, n_kv)
        send[peer] = partial(peer).astype(send.dtype)
        remote(send.at[peer], recv.at[me], rs_s.at[peer], rs_r.at[me], "kv", peer).start()
        return carry

    lax.fori_loop(1, n_kv, spread, 0)
    own = partial(me)
    collect(stat, stat_s, stat_r, "kv", n_kv)
    stats = total_over(stat, n_kv)
    factor = lax.rsqrt(stats[0][:, :1] / d_total + EPSILON)
    logits = factor * stats[1][:, :heads] + bias_ref[...]
    gates_ref[...] = jnp.minimum(logits, 0.0) - jnp.log1p(jnp.exp(-jnp.abs(logits)))

    def gather(k, so_far):
        peer = lax.rem(me + k, n_kv)
        remote(send.at[peer], recv.at[peer], rs_s.at[peer], rs_r.at[peer], "kv", peer).wait_recv()
        return so_far + recv[peer].astype(F32)

    mine[me] = (factor * lax.fori_loop(1, n_kv, gather, own)).astype(BF16)
    share(mine, ag_s, ag_r, "kv", n_kv)
    collect(mine, ag_s, ag_r, "kv", n_kv)
    for j in range(-(-3 * each // width)):
        out_ref[:, j * width : (j + 1) * width] = mine[j]

    def sent(k, carry):
        peer = lax.rem(me + k, n_kv)
        remote(send.at[peer], recv.at[me], rs_s.at[peer], rs_r.at[me], "kv", peer).wait_send()
        return carry

    lax.fori_loop(1, n_kv, sent, 0)
    drain(stat, stat_s, stat_r, "kv", n_kv)
    drain(mine, ag_s, ag_r, "kv", n_kv)


def project(tokens, gain, query, key, value, forget, bias):
    n_kv, n_tp = lax.axis_size("kv"), lax.axis_size("tp")
    rows, features = tokens.shape
    total = 3 * query.shape[1]
    width = chunk_width(total, n_kv)
    padded = width * n_kv
    columns = width * (-(-total // width))
    heads = forget.shape[1]
    return pl.pallas_call(
        functools.partial(project_kernel, n_kv, n_tp, width, float(features * n_kv)),
        out_shape=(
            jax.ShapeDtypeStruct((rows, columns), BF16),
            jax.ShapeDtypeStruct((rows, heads), F32),
        ),
        in_specs=[VM, VM, ANY, ANY, ANY, VM, VM],
        out_specs=(VM, VM),
        scratch_shapes=[
            pltpu.VMEM((features, padded), BF16),
            pltpu.VMEM((n_kv, 2, rows, LANES), F32),
            pltpu.VMEM((n_kv, rows, width), F32),
            pltpu.VMEM((n_kv, rows, width), F32),
            pltpu.VMEM((n_kv, rows, width), BF16),
            DMA((3,)),
            DMA((n_kv,)), DMA((n_kv,)),
            DMA((n_kv,)), DMA((n_kv,)),
            DMA((n_kv,)), DMA((n_kv,)),
        ],
        compiler_params=pltpu.CompilerParams(
            collective_id=1, has_side_effects=True, vmem_limit_bytes=24 << 20
        ),
        name="project",
    )(tokens, gain.reshape(1, features), query, key, value, forget, bias.reshape(1, heads))


def attend_kernel(inverse, q_ref, bias_ref, k_ref, v_ref, num_ref, top_ref, den_ref):
    heads = q_ref.shape[1]
    spots = k_ref.shape[1]
    head_of = lax.broadcasted_iota(jnp.int32, (heads, spots), 0)
    spot_of = lax.broadcasted_iota(jnp.int32, (heads, spots), 1)
    same = lax.rem(spot_of, heads) == head_of
    for i in range(q_ref.shape[0]):
        scores = lax.dot_general(
            q_ref[i], k_ref[i], (((1,), (1,)), ((), ())), preferred_element_type=F32
        )
        scores = jnp.where(same, scores * inverse + bias_ref[i], -jnp.inf)
        top = jnp.max(scores, axis=1, keepdims=True)
        weights = jnp.exp(scores - top).astype(BF16)
        den = jnp.sum(weights.astype(F32), axis=1, keepdims=True)
        num_ref[i] = jnp.dot(weights, v_ref[i], preferred_element_type=F32)
        top_ref[i] = jnp.broadcast_to(top, (heads, LANES))
        den_ref[i] = jnp.broadcast_to(den, (heads, LANES))


def attend(query, bias, keys, values):
    count, heads, size = query.shape
    spots = keys.shape[1]
    group = 2 if count % 2 == 0 else 1
    at = lambda b: (b, 0, 0)
    result = jax.ShapeDtypeStruct((count, heads, size), F32)
    stat = jax.ShapeDtypeStruct((count, heads, LANES), F32)
    return pl.pallas_call(
        functools.partial(attend_kernel, size ** (-0.5)),
        grid=(count // group,),
        out_shape=(result, stat, stat),
        in_specs=[
            pl.BlockSpec((group, heads, size), at),
            pl.BlockSpec((group, 1, spots), at),
            pl.BlockSpec((group, spots, size), at),
            pl.BlockSpec((group, spots, size), at),
        ],
        out_specs=(
            pl.BlockSpec((group, heads, size), at),
            pl.BlockSpec((group, heads, LANES), at),
            pl.BlockSpec((group, heads, LANES), at),
        ),
        compiler_params=pltpu.CompilerParams(vmem_limit_bytes=32 << 20),
        name="attend",
    )(query, bias, keys, values)


def merge_kernel(
    n_kv, n_tp, part_count, inverse,
    tokens_ref, num_ref, top_ref, den_ref, q_ref, k_ref, v_ref, gate_ref, w_ref, out_ref,
    send, recv, att, tp_buf,
    rs_s, rs_r, ag_s, ag_r, tp_s, tp_r,
):
    me = lax.axis_index("kv")
    count, heads = num_ref.shape[0], num_ref.shape[1]
    for i in range(n_kv):
        low, high = i * part_count, min((i + 1) * part_count, count)
        if high - low < part_count:
            send[i] = jnp.zeros(send.shape[1:], F32)
        if high > low:
            send[i, 0, : high - low] = num_ref[low:high]
            send[i, 1, : high - low] = top_ref[low:high]
            send[i, 2, : high - low] = den_ref[low:high]
    greet(n_kv, n_tp)

    def spread(k, carry):
        peer = lax.rem(me + k, n_kv)
        remote(send.at[peer], recv.at[me], rs_s.at[peer], rs_r.at[me], "kv", peer).start()
        return carry

    lax.fori_loop(1, n_kv, spread, 0)
    mine = pl.ds(me * part_count, part_count)
    query = q_ref[mine].astype(F32)
    own = jnp.sum(query * k_ref[mine].astype(F32), axis=2, keepdims=True) * inverse
    log_gate = gate_ref[mine]

    def gather(k, so_far):
        peer = lax.rem(me + k, n_kv)
        remote(send.at[peer], recv.at[peer], rs_s.at[peer], rs_r.at[peer], "kv", peer).wait_recv()
        num, top, den = so_far
        high = jnp.maximum(top, recv[peer, 1])
        old, new = jnp.exp(top - high), jnp.exp(recv[peer, 1] - high)
        return num * old + recv[peer, 0] * new, high, den * old + recv[peer, 2] * new

    num, top, den = lax.fori_loop(1, n_kv, gather, (send[me, 0], send[me, 1], send[me, 2]))
    top = top + log_gate
    ceiling = jnp.maximum(top, own)
    cache_scale, own_scale = jnp.exp(top - ceiling), jnp.exp(own - ceiling)
    attended = (num * cache_scale + own_scale * v_ref[mine].astype(F32)) / (
        den * cache_scale + own_scale
    )
    att[me] = attended.astype(BF16).astype(F32)
    share(att, ag_s, ag_r, "kv", n_kv)
    collect(att, ag_s, ag_r, "kv", n_kv)
    whole = att[...].reshape((n_kv * part_count, heads, LANES))[:count]
    size = LANES
    part = jnp.zeros((count, w_ref.shape[1]), F32)
    for h in range(heads):
        part += jnp.dot(
            whole[:, h, :].astype(BF16), w_ref[h * size : (h + 1) * size, :],
            preferred_element_type=F32,
        )
    summed = across_tp(part, tp_buf, tp_s, tp_r, n_tp)
    out_ref[...] = (tokens_ref[...].astype(F32) + summed).astype(BF16)

    def sent(k, carry):
        peer = lax.rem(me + k, n_kv)
        remote(send.at[peer], recv.at[me], rs_s.at[peer], rs_r.at[me], "kv", peer).wait_send()
        return carry

    lax.fori_loop(1, n_kv, sent, 0)
    drain(att, ag_s, ag_r, "kv", n_kv)
    drain(tp_buf, tp_s, tp_r, "tp", n_tp)


def merge(tokens, num, top, den, query, key, value, log_gate, out_weight):
    n_kv, n_tp = lax.axis_size("kv"), lax.axis_size("tp")
    rows, features = tokens.shape
    count, heads, size = num.shape
    part_count = -(-count // n_kv)
    pad = ((0, part_count * n_kv - count), (0, 0), (0, 0))
    query, key, value = (jnp.pad(x, pad) for x in (query, key, value))
    log_gate = jnp.pad(jnp.broadcast_to(log_gate[:, :, None], (count, heads, LANES)), pad)
    return pl.pallas_call(
        functools.partial(merge_kernel, n_kv, n_tp, part_count, size ** (-0.5)),
        out_shape=jax.ShapeDtypeStruct((rows, features), BF16),
        in_specs=[VM] * 9,
        out_specs=VM,
        scratch_shapes=[
            pltpu.VMEM((n_kv, 3, part_count, heads, LANES), F32),
            pltpu.VMEM((n_kv, 3, part_count, heads, LANES), F32),
            pltpu.VMEM((n_kv, part_count, heads, LANES), F32),
            pltpu.VMEM((n_tp, rows, features), BF16),
            DMA((n_kv,)), DMA((n_kv,)),
            DMA((n_kv,)), DMA((n_kv,)),
            DMA((n_tp,)), DMA((n_tp,)),
        ],
        compiler_params=pltpu.CompilerParams(
            collective_id=2, has_side_effects=True, vmem_limit_bytes=24 << 20
        ),
        name="merge",
    )(tokens, num, top, den, query, key, value, log_gate, out_weight)


def on_device(
    tokens,
    gain_first,
    gate_first,
    up_first,
    down_first,
    gain_mixer,
    query_weight,
    key_weight,
    value_weight,
    forget_weight,
    forget_bias,
    key_cache,
    value_cache,
    forget_sum,
    out_weight,
    gain_second,
    gate_second,
    up_second,
    down_second,
):
    count, spots, heads, size = key_cache.shape
    bias = forget_sum.transpose(0, 2, 1).reshape(count, 1, spots * heads)
    first_out = feed_forward(tokens, gain_first, gate_first, up_first, down_first, 0)
    projected, all_gates = project(
        first_out, gain_mixer, query_weight, key_weight, value_weight, forget_weight, forget_bias
    )
    each = heads * size
    query, new_key, new_value = (
        projected[:, i * each : (i + 1) * each].reshape(count, heads, size) for i in range(3)
    )
    log_gate = lax.dynamic_slice_in_dim(all_gates, lax.axis_index("tp") * heads, heads, 1)
    num, top, den = attend(
        query,
        bias,
        key_cache.reshape(count, spots * heads, size),
        value_cache.reshape(count, spots * heads, size),
    )
    mixed = merge(first_out, num, top, den, query, new_key, new_value, log_gate, out_weight)
    return feed_forward(mixed, gain_second, gate_second, up_second, down_second, 3)


def solution(mesh):
    in_specs = (
        P(None, "kv"),
        P("kv"),
        P("kv", "tp"),
        P("kv", "tp"),
        P("tp", "kv"),
        P("kv"),
        P("kv", "tp"),
        P("kv", "tp"),
        P("kv", "tp"),
        P(),
        P(),
        P(None, "kv", "tp", None),
        P(None, "kv", "tp", None),
        P(None, "tp", "kv"),
        P("tp", "kv"),
        P("kv"),
        P("kv", "tp"),
        P("kv", "tp"),
        P("tp", "kv"),
    )
    return jax.shard_map(
        on_device, mesh=mesh, in_specs=in_specs, out_specs=P(None, "kv"), check_vma=False
    )
```

time: 538 us -> 163 us (0.30)
  waiting for transfers between devices: 250 us -> 0 us
  blocking collectives: 209 us -> 0 us
  Pallas kernels: 0 us -> 145 us
  matrix products: 36.3 us -> 0 us
  other arithmetic: 23.5 us -> 0 us
  between operations: 13.4 us -> 0.31 us
  local copies, waits for them, and re-layouts: 4.77 us -> 16.6 us
    psum x3 -> x0, waiting for transfers between devices: 250 us -> none  [the longest x2 146 us: feed_forward(): products, squares = lax.psum((products, squares), 'kv')]
    pallas_call x0 -> x5, Pallas kernels: none -> 145 us  [the longest x2 68.3 us: feed_forward(): pl.pallas_call(functools.partial(feed_kernel, n_kv, n_tp, width, float(fe...]
    psum x6 -> x0, blocking collectives: 134 us -> none  [the longest x2 83.1 us: feed_forward(): products, squares = lax.psum((products, squares), 'kv')]
    all_gather x2 -> x0, blocking collectives: 75.2 us -> none  [combined_all(): everything = jax.tree.map(lambda part: lax.all_gather(part, axis), value)]
    dot_general x13 -> x0, matrix products: 36.3 us -> none  [the longest x1 11.6 us: mix_tokens(): jnp.einsum('bhd,bshd->bhs', query_rows, key_cache, preferred_element_type...]
    add x31 -> x0, other arithmetic: 15.7 us -> none  [the longest x15 15.4 us: merge_parts(): former[2] * left_scale[..., None] + latter[2] * right_scale[..., None]]
    unnamed x29 -> x46, local copies, waits for them, and re-layouts: 1.25 us -> 14.1 us
  transfers between devices with their start and end apart: 4 -> 0, of which waited for: 3 -> 0; matrix products, arithmetic and copies ran while one was open for 0% -> 0% of each run, Pallas kernels for 0% -> 0%
where the time goes in v1:
time: 163 us; the launch traced here: 162 us
  Pallas kernels  145 us (89%)
  local copies, waits for them, and re-layouts  16.6 us (10%)
    pallas_call x2, Pallas kernels, feed_forward(): pl.pallas_call(functools.partial(feed_kernel, n_kv, n_tp, width, float(fe...  68.3 us
    pallas_call x1, Pallas kernels, project(): pl.pallas_call(functools.partial(project_kernel, n_kv, n_tp, width, float...  31.5 us
    pallas_call x1, Pallas kernels, attend(): pl.pallas_call(functools.partial(attend_kernel, size ** (-0.5)), grid=(co...  23.5 us
    pallas_call x1, Pallas kernels, merge(): pl.pallas_call(functools.partial(merge_kernel, n_kv, n_tp, part_count, si...  21.7 us
    unnamed x46, local copies, waits for them, and re-layouts  14.1 us

profile of v1, /device:TPU:0, one launch (start us, length us, event | category | flops | bytes accessed | tf_op | source)
XLA Modules:
  0.0 161.9 jit_solution(11294965895904239041)
XLA Ops:
  0.0 0.7 reshape.31.gain_ref
  0.7 1.8 %copy-done = bf16[256,5632]{1,0:T(8,128)(2,1)S(1)} copy-done((bf16[256,5632]{1,0:T(8,128)(2,1)S(1)}, bf16[256,5632]{1,0:T(8,128)(2,1)}, u32[]{:S(2)}) %copy-start) | copy-done | bytes 2883608
  2.5 1.8 %copy-done.1 = bf16[256,5632]{1,0:T(8,128)(2,1)S(1)} copy-done((bf16[256,5632]{1,0:T(8,128)(2,1)S(1)}, bf16[256,5632]{1,0:T(8,128)(2,1)}, u32[]{:S(2)}) %copy-start.1) | copy-done | bytes 2883608
  4.3 1.8 %copy-done.2 = bf16[5632,256]{1,0:T(8,128)(2,1)S(1)} copy-done((bf16[5632,256]{1,0:T(8,128)(2,1)S(1)}, bf16[5632,256]{1,0:T(8,128)(2,1)}, u32[]{:S(2)}) %copy-start.2) | copy-done | bytes 2883608
  6.1 0.7 copy-done.12
  6.8 0.0 copy-start.9
  6.8 0.0 copy-start.13
  6.8 37.9 %feed_0.1.tokens_ref = bf16[24,256]{1,0:T(8,128)(2,1)S(1)} custom-call(bf16[24,256]{1,0:T(8,128)(2,1)S(1)} %copy-done.12, bf16[1,256]{1,0:T(2,128)(2,1)S(1)} %reshape.31.gain_ref, bf16[256,5632]{1,0:T(8,128)(2,1)S(1)} %copy-done, bf16[256,5632]{1,0:T(8,128)(2,1)S(1)} %copy-done.1, bf16[5632,256]{1,0:T(8,128)(2,1)S(1)} %copy-done.2), custom_call_target="tpu_custom_call" | custom-call | tf_op jit(solution)/shard_map/feed_0/pallas_call | solution.py:197
  44.7 0.0 copy-done.18
  44.7 0.0 copy-start.14
  44.8 0.0 copy-done.17
  44.8 0.5 copy.22.forget_ref
  45.3 31.5 %project.1 = (bf16[24,3072]{1,0:T(8,128)(2,1)S(1)}, f32[24,16]{1,0:T(8,128)S(1)}) custom-call(bf16[24,256]{1,0:T(8,128)(2,1)S(1)} %feed_0.1.tokens_ref, bf16[1,256]{1,0:T(2,128)(2,1)S(1)} %reshape.32.gain_ref, bf16[256,1024]{1,0:T(8,128)(2,1)S(1)} %copy-done.7, bf16[256,1024]{1,0:T(8,128)(2,1)S(1)} %copy-done.8, bf16[256,1024]{1,0:T(8,128)(2,1)S(1)} %copy-done.9, ...), custom_call_target="tpu_custom_call" | custom-call | tf_op jit(solution)/shard_map/project/pallas_call | solution.py:301
  76.8 0.7 slice_bitcast_fusion
  77.5 0.8 copy.23
  78.3 0.8 copy.24.bias_ref
  79.2 0.0 copy-start.19
  79.2 0.0 copy-start.3
  79.2 23.5 %attend.1 = (f32[24,8,128]{2,1,0:T(8,128)S(1)}, f32[24,8,128]{2,1,0:T(8,128)S(1)}, f32[24,8,128]{2,1,0:T(8,128)S(1)}) custom-call(bf16[24,8,128]{2,1,0:T(8,128)(2,1)S(1)} %bitcast.14, f32[24,1,4096]{2,1,0:T(1,128)S(1)} %copy.24.bias_ref, bf16[24,4096,128]{2,1,0:T(8,128)(2,1)} %bitcast.17, bf16[24,4096,128]{2,1,0:T(8,128)(2,1)} %bitcast.18), custom_call_target="tpu_custom_call" | custom-call | tf_op jit(solution)/shard_map/attend/pallas_call | solution.py:353
  102.8 0.0 copy-done.15
  102.8 0.6 copy-done.10
  103.3 0.1 constant_dynamic-slice_fusion
  103.4 0.1 broadcast_in_dim.2
  103.5 0.0 copy-start.6
  103.5 1.0 copy-done.6
  104.6 0.9 copy-done.11
  105.5 21.7 %merge.1.tokens_ref = bf16[24,256]{1,0:T(8,128)(2,1)S(1)} custom-call(bf16[24,256]{1,0:T(8,128)(2,1)S(1)} %feed_0.1.tokens_ref, f32[24,8,128]{2,1,0:T(8,128)S(1)} %get-tuple-element.11.num_ref, f32[24,8,128]{2,1,0:T(8,128)S(1)} %get-tuple-element.12.top_ref, f32[24,8,128]{2,1,0:T(8,128)S(1)} %copy-done.11, bf16[32,8,128]{2,1,0:T(8,128)(2,1)S(1)} %pad.14.q_ref, ...), custom_call_target="tpu_custom_call" | custom-call | tf_op jit(solution)/shard_map/merge/pallas_call | solution.py:449
  127.2 0.0 copy-start.4
  127.2 1.8 %copy-done.4 = bf16[256,5632]{1,0:T(8,128)(2,1)S(1)} copy-done((bf16[256,5632]{1,0:T(8,128)(2,1)S(1)}, bf16[256,5632]{1,0:T(8,128)(2,1)}, u32[]{:S(2)}) %copy-start.4) | copy-done | bytes 2883608
  129.0 1.8 %copy-done.5 = bf16[5632,256]{1,0:T(8,128)(2,1)S(1)} copy-done((bf16[5632,256]{1,0:T(8,128)(2,1)S(1)}, bf16[5632,256]{1,0:T(8,128)(2,1)}, u32[]{:S(2)}) %copy-start.5) | copy-done | bytes 2883608
  130.8 30.4 %feed_3.1 = bf16[24,256]{1,0:T(8,128)(2,1)S(1)} custom-call(bf16[24,256]{1,0:T(8,128)(2,1)S(1)} %merge.1.tokens_ref, bf16[1,256]{1,0:T(2,128)(2,1)S(1)} %reshape.40.gain_ref, bf16[256,5632]{1,0:T(8,128)(2,1)S(1)} %copy-done.3, bf16[256,5632]{1,0:T(8,128)(2,1)S(1)} %copy-done.4, bf16[5632,256]{1,0:T(8,128)(2,1)S(1)} %copy-done.5), custom_call_target="tpu_custom_call" | custom-call | tf_op jit(solution)/shard_map/feed_3/pallas_call | solution.py:197
  161.2 0.6 copy.29
  (30 shorter events, 0.1 us)
Async XLA Ops:
  0.7 1.8 %copy-start = (bf16[256,5632]{1,0:T(8,128)(2,1)S(1)}, bf16[256,5632]{1,0:T(8,128)(2,1)}, u32[]{:S(2)}) copy-start(bf16[256,5632]{1,0:T(8,128)(2,1)} %gate_hbm.2) | copy-start | bytes 8650756
  2.5 1.8 %copy-start.1 = (bf16[256,5632]{1,0:T(8,128)(2,1)S(1)}, bf16[256,5632]{1,0:T(8,128)(2,1)}, u32[]{:S(2)}) copy-start(bf16[256,5632]{1,0:T(8,128)(2,1)} %up_hbm.2) | copy-start | bytes 8650756
  4.3 1.8 %copy-start.2 = (bf16[5632,256]{1,0:T(8,128)(2,1)S(1)}, bf16[5632,256]{1,0:T(8,128)(2,1)}, u32[]{:S(2)}) copy-start(bf16[5632,256]{1,0:T(8,128)(2,1)} %down_hbm.2) | copy-start | bytes 8650756
  6.1 0.7 copy-start.12
  6.8 37.9 %copy-start.18 = (bf16[256]{0:T(256)(128)(2,1)S(1)}, bf16[256]{0:T(256)(128)(2,1)}, u32[]{:S(2)}) copy-start(bf16[256]{0:T(256)(128)(2,1)} %param.24) | copy-start | bytes 1540
  6.8 38.0 %copy-start.17 = (bf16[4096,16]{0,1:T(8,128)(2,1)S(1)}, bf16[4096,16]{0,1:T(8,128)(2,1)}, u32[]{:S(2)}) copy-start(bf16[4096,16]{0,1:T(8,128)(2,1)} %param.28) | copy-start | bytes 393220
  6.8 38.4 %copy-start.7 = (bf16[256,1024]{1,0:T(8,128)(2,1)S(1)}, bf16[256,1024]{1,0:T(8,128)(2,1)}, u32[]{:S(2)}) copy-start(bf16[256,1024]{1,0:T(8,128)(2,1)} %query_hbm.1) | copy-start | bytes 1572868
  6.8 38.4 %copy-start.8 = (bf16[256,1024]{1,0:T(8,128)(2,1)S(1)}, bf16[256,1024]{1,0:T(8,128)(2,1)}, u32[]{:S(2)}) copy-start(bf16[256,1024]{1,0:T(8,128)(2,1)} %key_hbm.1) | copy-start | bytes 1572868
  6.8 38.5 %copy-start.9 = (bf16[256,1024]{1,0:T(8,128)(2,1)S(1)}, bf16[256,1024]{1,0:T(8,128)(2,1)}, u32[]{:S(2)}) copy-start(bf16[256,1024]{1,0:T(8,128)(2,1)} %value_hbm.1) | copy-start | bytes 1572868
  6.8 38.5 %copy-start.13 = (f32[16]{0:T(128)S(1)}, f32[16]{0:T(128)}, u32[]{:S(2)}) copy-start(f32[16]{0:T(128)} %param.29) | copy-start | bytes 196
  44.7 32.8 %copy-start.14 = (f32[24,8,512]{2,1,0:T(8,128)S(1)}, f32[24,8,512]{2,1,0:T(8,128)}, u32[]{:S(2)}) copy-start(f32[24,8,512]{2,1,0:T(8,128)} %param.32) | copy-start | bytes 1179652
  79.2 23.5 %copy-start.16 = (bf16[3,8,8,128]{3,1,2,0:T(8,128)(2,1)S(1)}, bf16[3,8,8,128]{3,1,2,0:T(8,128)(2,1)}, u32[]{:S(2)}) copy-start(bf16[3,8,8,128]{3,1,2,0:T(8,128)(2,1)} %get-tuple-element.16) | copy-start | bytes 147460
  79.2 23.6 %copy-start.15 = (bf16[3,8,8,128]{3,1,2,0:T(8,128)(2,1)S(1)}, bf16[3,8,8,128]{3,1,2,0:T(8,128)(2,1)}, u32[]{:S(2)}) copy-start(bf16[3,8,8,128]{3,1,2,0:T(8,128)(2,1)} %get-tuple-element.15) | copy-start | bytes 147460
  79.2 47.9 %copy-start.19 = (bf16[256]{0:T(256)(128)(2,1)S(1)}, bf16[256]{0:T(256)(128)(2,1)}, u32[]{:S(2)}) copy-start(bf16[256]{0:T(256)(128)(2,1)} %param.34) | copy-start | bytes 1540
  79.2 47.9 %copy-start.3 = (bf16[256,5632]{1,0:T(8,128)(2,1)S(1)}, bf16[256,5632]{1,0:T(8,128)(2,1)}, u32[]{:S(2)}) copy-start(bf16[256,5632]{1,0:T(8,128)(2,1)} %gate_hbm.3) | copy-start | bytes 8650756
  102.7 0.6 copy-start.10
  103.5 1.0 copy-start.6
  104.6 0.9 copy-start.11
  127.2 1.8 %copy-start.4 = (bf16[256,5632]{1,0:T(8,128)(2,1)S(1)}, bf16[256,5632]{1,0:T(8,128)(2,1)}, u32[]{:S(2)}) copy-start(bf16[256,5632]{1,0:T(8,128)(2,1)} %up_hbm.3) | copy-start | bytes 8650756
  129.0 1.8 %copy-start.5 = (bf16[5632,256]{1,0:T(8,128)(2,1)S(1)}, bf16[5632,256]{1,0:T(8,128)(2,1)}, u32[]{:S(2)}) copy-start(bf16[5632,256]{1,0:T(8,128)(2,1)} %down_hbm.3) | copy-start | bytes 8650756
